TPU v7x, 32 devices: a whole 2x2x4 slice. The times are simulated.
32 devices in a mesh: grp: 2 (over y), dp: 2 (over x), kv: 4 (over z), tp: 2 (over core).
Axes of the slice: x: 2, y: 2, z: 4, core: 2. Of those that a mesh axis runs over, the one named last changes fastest.
Arguments:
- tokens: bfloat16 [128, 2048], P(('grp', 'dp'), ('kv', 'tp')), parts along dimension 0, may hold values from -6 to 6
- norm_gain: float32 [2048], P('kv'), may hold values from 0.1 to 1.9
- w_query: bfloat16 [2048, 512], P('kv', 'tp'), may hold values from -0.125 to 0.125
- w_key: bfloat16 [2048, 512], P('kv', 'tp'), may hold values from -0.125 to 0.125
- w_value: bfloat16 [2048, 1024], P('kv', 'tp'), may hold values from -0.125 to 0.125
- w_outgate: bfloat16 [2048, 1024], P('kv', 'tp'), may hold values from -0.125 to 0.125
- w_ingate: bfloat16 [2048, 8], P('kv'), may hold values from -0.125 to 0.125
- w_forget: bfloat16 [2048, 8], P('kv'), may hold values from -0.125 to 0.125
- in_bias: float32 [8], replicated, may hold values from -1.5 to 0.5
- forget_bias: float32 [8], replicated, may hold values from -1 to 4
- memory: float32 [128, 8, 64, 128], P(('grp', 'dp', 'kv'), 'tp'), parts along dimension 0, may hold values from -4 to 4
- normalizer: float32 [128, 512], P(('grp', 'dp', 'kv'), 'tp'), parts along dimension 0, may hold values from -4 to 4
- stabilizer: float32 [128, 8], P(('grp', 'dp', 'kv'), 'tp'), parts along dimension 0, may hold values from -1 to 1
- w_out: bfloat16 [1024, 2048], P('tp', 'kv'), may hold values from -0.1875 to 0.1875
- mlp_gain: float32 [2048], replicated, may hold values from 0.1 to 1.9
- w_up: bfloat16 [2048, 8192], P(None, ('kv', 'tp')), may hold values from -0.125 to 0.125
- w_down: bfloat16 [8192, 2048], P(('kv', 'tp')), may hold values from -0.09375 to 0.09375
Outputs:
- mixed_out: bfloat16 [128, 2048], P(('grp', 'dp'), ('kv', 'tp')), parts along dimension 0
- memory_new: float32 [128, 8, 64, 128], P(('grp', 'dp', 'kv'), 'tp'), parts along dimension 0
- normalizer_new: float32 [128, 512], P(('grp', 'dp', 'kv'), 'tp'), parts along dimension 0
- stabilizer_new: float32 [128, 8], P(('grp', 'dp', 'kv'), 'tp'), parts along dimension 0
There are 2 independent parts, one for each index of `grp`. A program takes and returns all parts, laid end to end along the dimension named above; an argument that names none is the same for every part. Nothing has to cross between parts.
All inputs are finite; a program needn't handle non-finite values.
Results may differ from a plain program's by a relative error of at most 0.03.
Values may be sent and summed in bfloat16 or wider, within the bound.
A program may use at most 64 MiB of HBM per device.

v0:
```python
import jax
import jax.numpy as jnp
from jax import lax
from jax.sharding import PartitionSpec as P

EPSILON = 1e-06


def channel_mix(rows_in, mlp_gain, w_up, w_down):
    rows_f = rows_in.astype(jnp.float32)
    rscale_mid = lax.rsqrt(jnp.mean(rows_f * rows_f, axis=1, keepdims=True) + EPSILON)
    normed = (rows_f * rscale_mid * mlp_gain).astype(jnp.bfloat16)
    upward = jnp.dot(normed, w_up, preferred_element_type=jnp.float32)
    squared = jnp.square(jax.nn.relu(upward)).astype(jnp.bfloat16)
    return jnp.dot(squared, w_down, preferred_element_type=jnp.float32).astype(jnp.bfloat16)


def shards(
    tokens,
    norm_gain,
    w_query,
    w_key,
    w_value,
    w_outgate,
    w_ingate,
    w_forget,
    in_bias,
    forget_bias,
    memory,
    normalizer,
    stabilizer,
    w_out,
    mlp_gain,
    w_up,
    w_down,
):
    local_heads = memory.shape[1]
    qk_width = memory.shape[2]
    model_width = mlp_gain.shape[0]
    own_rows = lax.all_gather(tokens, "tp", axis=1, tiled=True)
    own_f = own_rows.astype(jnp.float32)
    scaled = (own_f * norm_gain).astype(jnp.bfloat16)

    def product(weight):
        return jnp.dot(scaled, weight, preferred_element_type=jnp.float32).astype(jnp.bfloat16)

    part_query = product(w_query)
    part_key = product(w_key)
    part_value = product(w_value)
    part_gate = product(w_outgate)
    part_input = product(w_ingate)
    part_forget = product(w_forget)
    part_squares = jnp.sum(own_f * own_f, axis=1, keepdims=True)
    upper_piece = part_squares.astype(jnp.bfloat16)
    rest_one = part_squares - upper_piece.astype(jnp.float32)
    middle_piece = rest_one.astype(jnp.bfloat16)
    lower_piece = (rest_one - middle_piece.astype(jnp.float32)).astype(jnp.bfloat16)
    pieces = jnp.concatenate([upper_piece, middle_piece, lower_piece], axis=1)
    sum_query, sum_key, sum_value, sum_gate, sum_input, sum_forget, square_parts = (
        lax.psum_scatter(part_query, "kv", scatter_dimension=0, tiled=True).astype(jnp.float32),
        lax.psum_scatter(part_key, "kv", scatter_dimension=0, tiled=True).astype(jnp.float32),
        lax.psum_scatter(part_value, "kv", scatter_dimension=0, tiled=True).astype(jnp.float32),
        lax.psum_scatter(part_gate, "kv", scatter_dimension=0, tiled=True).astype(jnp.float32),
        lax.psum_scatter(part_input, "kv", scatter_dimension=0, tiled=True).astype(jnp.float32),
        lax.psum_scatter(part_forget, "kv", scatter_dimension=0, tiled=True).astype(jnp.float32),
        lax.psum_scatter(pieces, "kv", scatter_dimension=0, tiled=True).astype(jnp.float32),
    )
    squares = jnp.sum(square_parts, axis=1)
    seq_rows = sum_query.shape[0]
    rscale = lax.rsqrt(squares / model_width + EPSILON)[:, None]
    queries = (sum_query * rscale).reshape(seq_rows, local_heads, qk_width)
    keys_in = (sum_key * rscale * qk_width ** (-0.5)).reshape(seq_rows, local_heads, qk_width)
    values_in = (sum_value * rscale).reshape(seq_rows, local_heads, -1)
    out_pre = (sum_gate * rscale).reshape(seq_rows, local_heads, -1)
    head_first = lax.axis_index("tp") * local_heads
    log_in = lax.dynamic_slice_in_dim(
        sum_input * rscale, head_first, local_heads, 1
    ) + lax.dynamic_slice_in_dim(in_bias, head_first, local_heads, 0)
    forget_arg = lax.dynamic_slice_in_dim(
        sum_forget * rscale, head_first, local_heads, 1
    ) + lax.dynamic_slice_in_dim(forget_bias, head_first, local_heads, 0)
    log_forget = jax.nn.log_sigmoid(forget_arg)
    carried = log_forget + stabilizer
    stab_new = jnp.maximum(carried, log_in)
    take_new = jnp.exp(log_in - stab_new)
    keep_old = jnp.exp(carried - stab_new)
    norm_old = normalizer.reshape(seq_rows, local_heads, qk_width)
    score = jnp.sum(queries * keys_in, axis=2)
    readout = jnp.einsum("shkv,shk->shv", memory, queries, precision=lax.Precision.HIGHEST)
    numer = (take_new * score)[..., None] * values_in + keep_old[..., None] * readout
    denom = take_new * score + keep_old * jnp.sum(norm_old * queries, axis=2)
    cell = numer / jnp.maximum(jnp.abs(denom), 1.0)[..., None]
    hidden = (jax.nn.sigmoid(out_pre) * cell).reshape(seq_rows, -1).astype(jnp.bfloat16)
    memory_new = (
        keep_old[..., None, None] * memory
        + take_new[..., None, None] * keys_in[..., :, None] * values_in[..., None, :]
    )
    normalizer_new = (keep_old[..., None] * norm_old + take_new[..., None] * keys_in).reshape(
        seq_rows, -1
    )
    head_terms = jnp.dot(
        lax.all_gather(hidden, "kv", axis=0, tiled=True), w_out, preferred_element_type=jnp.float32
    )
    head_total = lax.psum_scatter(
        head_terms.astype(jnp.bfloat16), "tp", scatter_dimension=1, tiled=True
    ).astype(jnp.float32)
    middle = (tokens.astype(jnp.float32) + head_total).astype(jnp.bfloat16)
    whole_mid = lax.all_gather(middle, ("kv", "tp"), axis=1, tiled=True)
    branch = lax.psum_scatter(
        channel_mix(whole_mid, mlp_gain, w_up, w_down),
        ("kv", "tp"),
        scatter_dimension=1,
        tiled=True,
    ).astype(jnp.float32)
    mixed_out = (middle.astype(jnp.float32) + branch).astype(jnp.bfloat16)
    return (mixed_out, memory_new, normalizer_new, stab_new)


def solution(mesh):
    placed = (
        P(("grp", "dp"), ("kv", "tp")),
        P("kv"),
        P("kv", "tp"),
        P("kv", "tp"),
        P("kv", "tp"),
        P("kv", "tp"),
        P("kv", None),
        P("kv", None),
        P(),
        P(),
        P(("grp", "dp", "kv"), "tp", None, None),
        P(("grp", "dp", "kv"), "tp"),
        P(("grp", "dp", "kv"), "tp"),
        P("tp", "kv"),
        P(),
        P(None, ("kv", "tp")),
        P(("kv", "tp"), None),
    )
    return jax.shard_map(
        shards,
        mesh=mesh,
        in_specs=placed,
        out_specs=(
            P(("grp", "dp"), ("kv", "tp")),
            P(("grp", "dp", "kv"), "tp", None, None),
            P(("grp", "dp", "kv"), "tp"),
            P(("grp", "dp", "kv"), "tp"),
        ),
        check_vma=False,
    )
```

profile of v0, /device:TPU:0, one launch (start us, length us, event | category | flops | bytes accessed | tf_op | source)
XLA Modules:
  0.0 175.6 jit_solution(5340652048015191799)
XLA Ops:
  7.2 2.3 %all_gather.9 = bf16[32,512]{1,0:T(8,128)(2,1)S(1)} all-gather(bf16[32,256]{1,0:T(8,128)(2,1)} %param.17), channel_id=1, replica_groups=mesh['grp'=2,'dp'=2,'kv'=4,'tp'=2] {'tp'}, dimensions={1}, use_global_device_ids=true | all-gather | bytes 49152 | tf_op jit(solution)/shard_map/all_gather | solution.py:40
  9.6 1.7 convolution_convert_fusion.5
  11.4 1.7 convolution_convert_fusion.4
  13.2 1.5 convolution_convert_fusion.3
  14.7 1.9 %convolution_convert_fusion.2 = bf16[32,512]{1,0:T(8,128)(2,1)} fusion(bf16[512,512]{1,0:T(8,128)(2,1)} %param.21, bf16[32,512]{1,0:T(8,128)(2,1)S(1)} %all_gather.9, f32[512]{0:T(512)} %param.18), kind=kOutput, calls=%fused_computation.5 | convolution fusion | flops 16842752 | bytes 591872 | tf_op jit(solution)/shard_map/dot_general | solution.py:45
  16.8 0.7 dynamic_slice.13
  17.6 0.7 dynamic_slice.15
  18.3 0.8 copy.27
  19.0 0.8 reshape.108
  19.8 0.8 convolution_convert_fusion.7
  20.7 0.8 convolution_convert_fusion.6
  21.5 1.2 dynamic-slice
  23.4 20.5 %all-reduce.3 = (bf16[32,8]{1,0:T(8,128)(2,1)S(1)}, bf16[32,3]{0,1:T(4,128)(2,1)S(1)}, bf16[32,8]{1,0:T(8,128)(2,1)S(1)}) all-reduce(bf16[32,8]{1,0:T(8,128)(2,1)S(1)} %convolution_convert_fusion.7, bf16[32,3]{0,1:T(4,128)(2,1)S(1)} %pad_maximum_fusion, ...), channel_id=4, replica_groups=mesh['grp'=2,'dp'=2,'kv'=4,'tp'=2] {'kv'}, use_global_device_ids=true, to_apply=%region_4.0.clone | all-reduce | flops 608 | bytes 2432
  44.1 9.4 %reduce-scatter.12.cloned.1.call-done = bf16[8,256]{1,0:T(8,128)(2,1)} async-done(((bf16[32,256]{1,0:T(8,128)(2,1)}), bf16[8,256]{1,0:T(8,128)(2,1)}) %reduce-scatter.12.cloned.1.call-update) | async-done | bytes 4112 | tf_op jit(solution)/shard_map/reduce_scatter | solution.py:61
  53.5 0.8 multiply_multiply_fusion
  55.0 2.2 %fusion.31 = f32[8,4,1,128]{3,2,1,0:T(1,128)S(1)} fusion(f32[8,4,64,1]{2,3,1,0:T(1,128)S(1)} %bitcast.53, f32[8,4,64,128]{3,2,1,0:T(8,128)} %param.27), kind=kOutput, calls=%fused_computation.58 | convolution fusion | flops 3145728 | bytes 1073152 | tf_op jit(solution)/shard_map/shkv,shk->shv/dot_general | solution.py:89
  57.2 1.4 multiply_add_fusion.1
  58.9 0.7 copy.32
  59.6 14.2 %reduce-scatter.8.cloned.1.call-done = bf16[8,512]{1,0:T(8,128)(2,1)} async-done(((bf16[32,512]{1,0:T(8,128)(2,1)}), bf16[8,512]{1,0:T(8,128)(2,1)}) %reduce-scatter.8.cloned.1.call-update) | async-done | bytes 8208 | tf_op jit(solution)/shard_map/reduce_scatter | solution.py:63
  73.7 19.5 %reduce-scatter.14.cloned.1.call-done = bf16[8,512]{1,0:T(8,128)(2,1)} async-done(((bf16[32,512]{1,0:T(8,128)(2,1)}), bf16[8,512]{1,0:T(8,128)(2,1)}) %reduce-scatter.14.cloned.1.call-update) | async-done | bytes 8208 | tf_op jit(solution)/shard_map/reduce_scatter | solution.py:62
  93.2 0.8 fusion.24
  94.0 13.1 %all_gather.10 = bf16[32,512]{1,0:T(8,128)(2,1)S(1)} all-gather(bf16[8,512]{1,0:T(8,128)(2,1)S(1)} %fusion.24), channel_id=1, replica_groups=mesh['grp'=2,'dp'=2,'kv'=4,'tp'=2] {'kv'}, dimensions={0}, use_global_device_ids=true | all-gather | bytes 40960 | tf_op jit(solution)/shard_map/all_gather | solution.py:102
  107.2 1.9 %convolution_convert_fusion.1 = bf16[32,512]{1,0:T(8,128)(2,1)} fusion(bf16[32,512]{1,0:T(8,128)(2,1)S(1)} %all_gather.10, bf16[512,512]{1,0:T(8,128)(2,1)} %param.30), kind=kOutput, calls=%fused_computation.4 | convolution fusion | flops 16793600 | bytes 589824 | tf_op jit(solution)/shard_map/dot_general | solution.py:101
  109.1 0.8 multiply_bitcast_fusion
  109.9 5.0 %reduce-scatter.16.cloned.1.call-done = bf16[32,256]{1,0:T(8,128)(2,1)} async-done(((bf16[32,512]{1,0:T(8,128)(2,1)}), bf16[32,256]{1,0:T(8,128)(2,1)}) %reduce-scatter.16.cloned.1.call-update) | async-done | bytes 16400 | tf_op jit(solution)/shard_map/reduce_scatter | solution.py:104
  114.9 0.7 add_convert_fusion.1
  115.6 14.2 %all_gather.11 = bf16[32,2048]{1,0:T(8,128)(2,1)S(1)} all-gather(bf16[32,256]{1,0:T(8,128)(2,1)S(1)} %add_convert_fusion.1), channel_id=1, replica_groups=mesh['grp'=2,'dp'=2,'kv'=4,'tp'=2] {'kv','tp'}, dimensions={1}, use_global_device_ids=true | all-gather | bytes 147456 | tf_op jit(solution)/shard_map/all_gather | solution.py:108
  129.8 0.1 fusion.2
  130.0 5.8 %convolution_convert_fusion = bf16[32,2048]{1,0:T(8,128)(2,1)} fusion(bf16[1024,2048]{1,0:T(8,128)(2,1)} %param.33, bf16[2048,1024]{1,0:T(8,128)(2,1)} %param.32, bf16[32,2048]{1,0:T(8,128)(2,1)S(1)} %all_gather.11, f32[2048]{0:T(1024)S(1)} %copy-done.3, f32[32]{0:T(128)S(1)} %add_rsqrt_fusion), kind=kOutput, calls=%fused_computation | convolution fusion | flops 268861440 | bytes 8659072 | tf_op jit(solution)/shard_map/dot_general | solution.py:15
  135.8 1.4 multiply_add_fusion
  137.2 30.2 %reduce-scatter.18.cloned.1.call-done = bf16[32,256]{1,0:T(8,128)(2,1)} async-done(((bf16[32,2048]{1,0:T(8,128)(2,1)}), bf16[32,256]{1,0:T(8,128)(2,1)}) %reduce-scatter.18.cloned.1.call-update) | async-done | bytes 16400 | tf_op jit(solution)/shard_map/reduce_scatter | solution.py:109
  167.4 1.3 add_convert_fusion
  (43 shorter events, 1.8 us)
Async XLA Ops:
  7.2 6.0 %copy-start = (bf16[512,512]{1,0:T(8,128)(2,1)S(1)}, bf16[512,512]{1,0:T(8,128)(2,1)}, u32[]{:S(2)}) copy-start(bf16[512,512]{1,0:T(8,128)(2,1)} %param.22) | copy-start | bytes 1572868
  7.2 107.7 %copy-start.2 = (bf16[32,256]{1,0:T(8,128)(2,1)S(1)}, bf16[32,256]{1,0:T(8,128)(2,1)}, u32[]{:S(2)}) copy-start(bf16[32,256]{1,0:T(8,128)(2,1)} %param.17) | copy-start | bytes 49156
  7.2 122.8 %copy-start.3 = (f32[2048]{0:T(1024)S(1)}, f32[2048]{0:T(1024)}, u32[]{:S(2)}) copy-start(f32[2048]{0:T(1024)} %param.31) | copy-start | bytes 24580
  7.2 36.9 %reduce-scatter.10.cloned.1.call-start = ((), (), s32[]{:S(2)}) async-start(), calls=%async_computation.7 | async-start | bytes 20480 | tf_op jit(solution)/shard_map/reduce_scatter | solution.py:60
  11.3 42.2 %reduce-scatter.12.cloned.1.call-start = ((), (), s32[]{:S(2)}) async-start(), calls=%async_computation.8 | async-start | bytes 20480 | tf_op jit(solution)/shard_map/reduce_scatter | solution.py:61
  13.1 60.6 %reduce-scatter.8.cloned.1.call-start = ((), (), s32[]{:S(2)}) async-start(), calls=%async_computation.6 | async-start | bytes 40960 | tf_op jit(solution)/shard_map/reduce_scatter | solution.py:63
  14.7 78.5 %reduce-scatter.14.cloned.1.call-start = ((), (), s32[]{:S(2)}) async-start(), calls=%async_computation.9 | async-start | bytes 40960 | tf_op jit(solution)/shard_map/reduce_scatter | solution.py:62
  16.6 98.2 %reduce-scatter.16.cloned.1.call-start = ((), (), s32[]{:S(2)}) async-start(), calls=%async_computation.10 | async-start | bytes 49152 | tf_op jit(solution)/shard_map/reduce_scatter | solution.py:104
  109.0 58.4 %reduce-scatter.18.cloned.1.call-start = ((), (), s32[]{:S(2)}) async-start(), calls=%async_computation.11 | async-start | bytes 147456 | tf_op jit(solution)/shard_map/reduce_scatter | solution.py:109
  130.0 5.8 %copy-start.1 = (f32[8,4,64,128]{3,2,1,0:T(8,128)S(1)}, f32[8,4,64,128]{3,2,1,0:T(8,128)}, u32[]{:S(2)}) copy-start(f32[8,4,64,128]{3,2,1,0:T(8,128)} %param.27) | copy-start | bytes 3145732
Sparse Core Ops, SparseCore 0:
  11.4 21.7 reduce-scatter.9
  36.1 17.3 reduce-scatter.11
  56.3 17.3 reduce-scatter.7
  75.8 17.3 reduce-scatter.13
  109.2 5.6 reduce-scatter.15
  135.9 31.4 reduce-scatter.17
where the time goes:
time: 177 us; the launch traced here: 176 us
  waiting for transfers between devices  78.4 us (44%)
  blocking collectives  50.2 us (28%)
  matrix products  18.3 us (10%)
  between operations  14.9 us (8%)
  other arithmetic  7.84 us (4%)
  local copies, waits for them, and re-layouts  5.71 us (3%)
    reduce_scatter x1, waiting for transfers between devices, shards(): lax.psum_scatter(channel_mix(whole_mid, mlp_gain, w_up, w_down), ('kv', '...  30.2 us
    unnamed x1, blocking collectives  20.5 us
    reduce_scatter x1, waiting for transfers between devices, shards(): lax.psum_scatter(part_value, 'kv', scatter_dimension=0, tiled=True)  19.5 us
    all_gather x1, blocking collectives, shards(): whole_mid = lax.all_gather(middle, ('kv', 'tp'), axis=1, tiled=True)  14.2 us
    reduce_scatter x1, waiting for transfers between devices, shards(): lax.psum_scatter(part_gate, 'kv', scatter_dimension=0, tiled=True)  14.2 us
    all_gather x1, blocking collectives, shards(): lax.all_gather(hidden, 'kv', axis=0, tiled=True)  13.1 us
    reduce_scatter x1, waiting for transfers between devices, shards(): lax.psum_scatter(part_key, 'kv', scatter_dimension=0, tiled=True)  9.41 us
    dot_general x6, matrix products, product(): jnp.dot(scaled, weight, preferred_element_type=jnp.float32)  8.49 us
  transfers between devices with their start and end apart: 6, of which 5 were waited for; matrix products, arithmetic and copies ran while one was open for 11% of the time, Pallas kernels for 0%

commit v1 on v0

v1 whole, which is shorter than its diff:
```python
import functools

import jax
import jax.numpy as jnp
from jax import lax
from jax.experimental import pallas as pl
from jax.experimental.pallas import tpu as pltpu
from jax.sharding import PartitionSpec as P

EPSILON = 1e-06
F32 = jnp.float32
BF16 = jnp.bfloat16
MESH = pl.DeviceIdType.MESH
LANES = 128


def far_first(count):
    return sorted(range(1, count), key=lambda d: (-min(d, count - d), d))


def step_kernel(
    n_kv,
    n_tp,
    tokens,
    norm_gain,
    w_query,
    w_key,
    w_value,
    w_outgate,
    w_ingate,
    w_forget,
    in_bias,
    forget_bias,
    memory,
    normalizer,
    stabilizer,
    w_out,
    mlp_gain,
    w_up,
    w_down,
    mixed_out,
    memory_new,
    normalizer_new,
    stabilizer_new,
    tok,
    ngain,
    wq,
    wk,
    wv,
    wg,
    wi,
    wf,
    bias_i,
    bias_f,
    mem,
    nrm,
    stab,
    wo,
    mgain,
    wu,
    wd,
    part_out,
    part_in,
    gate_out,
    gate_in,
    readout,
    hid,
    mid,
    wide,
    down_out,
    down_in,
    mem_out,
    nrm_out,
    stab_out,
    mix_out,
    load_sem,
    store_sem,
    tok_send,
    tok_recv,
    wo_send,
    wo_recv,
    part_send,
    part_recv,
    gate_send,
    gate_recv,
    hid_send,
    hid_recv,
    mid_send,
    mid_recv,
    down_send,
    down_recv,
):
    kv = lax.axis_index("kv")
    tp = lax.axis_index("tp")
    me = kv * n_tp + tp
    rows, width = tokens.shape
    seqs, heads, qk, vd = memory.shape
    model_width = mlp_gain.shape[1]
    aligned = width % LANES == 0
    n_all = n_kv * n_tp

    def load(index, src, dst):
        copy = pltpu.make_async_copy(src, dst, load_sem.at[index])
        copy.start()
        return copy

    if aligned:
        own_cols = pl.ds(pl.multiple_of(tp * width, LANES), width)
        wo_local = w_out.at[:, own_cols]
    else:
        wo_local = w_out
    get_tok = load(0, tokens, tok.at[tp])
    get_ngain = load(1, norm_gain, ngain)
    get_proj = [
        load(2 + i, src, dst)
        for i, (src, dst) in enumerate(
            [
                (w_query, wq),
                (w_key, wk),
                (w_value, wv),
                (w_outgate, wg),
                (w_ingate, wi),
                (w_forget, wf),
            ]
        )
    ]
    get_cell = [
        load(8 + i, src, dst)
        for i, (src, dst) in enumerate(
            [
                (in_bias, bias_i),
                (forget_bias, bias_f),
                (stabilizer, stab),
                (normalizer, nrm),
                (memory, mem),
            ]
        )
    ]
    get_wo = load(13, wo_local, wo.at[tp])
    get_mgain = load(14, mlp_gain, mgain)
    get_up = load(15, w_up, wu)
    get_down = load(16, w_down, wd)

    offsets = [(dk, dt) for dk in far_first(n_kv) for dt in range(n_tp)]
    offsets += [(0, dt) for dt in range(1, n_tp)]

    def peer(dk, dt):
        return lax.rem(kv + dk, n_kv), lax.rem(tp + dt, n_tp)

    barrier = pltpu.get_barrier_semaphore()
    for dk, dt in offsets:
        pk, pt = peer(dk, dt)
        pl.semaphore_signal(barrier, inc=1, device_id={"kv": pk, "tp": pt}, device_id_type=MESH)
    get_tok.wait()
    pl.semaphore_wait(barrier, len(offsets))

    def remote(src, dst, send, recv, pk, pt):
        return pltpu.make_async_remote_copy(
            src_ref=src,
            dst_ref=dst,
            send_sem=send,
            recv_sem=recv,
            device_id={"kv": pk, "tp": pt},
            device_id_type=MESH,
        )

    sends = []
    for dt in range(1, n_tp):
        pt = lax.rem(tp + dt, n_tp)
        copy = remote(tok.at[tp], tok.at[tp], tok_send.at[dt], tok_recv.at[tp], kv, pt)
        copy.start()
        sends.append(copy)
    for dt in range(1, n_tp):
        pt = lax.rem(tp + dt, n_tp)
        if aligned:
            src = w_out.at[:, pl.ds(pl.multiple_of(pt * width, LANES), width)]
        else:
            src = w_out
        copy = remote(src, wo.at[tp], wo_send.at[dt], wo_recv.at[tp], kv, pt)
        copy.start()
        sends.append(copy)
    get_ngain.wait()
    for copy in get_proj:
        copy.wait()
    for dt in range(1, n_tp):
        pt = lax.rem(tp + dt, n_tp)
        remote(tok.at[pt], tok.at[pt], tok_send.at[dt], tok_recv.at[pt], kv, pt).wait_recv()

    scaled = []
    squares = jnp.zeros((rows, 1), F32)
    for t in range(n_tp):
        block = tok[t].astype(F32)
        squares = squares + jnp.sum(block * block, axis=1, keepdims=True)
        scaled.append((block * ngain[:, t * width : (t + 1) * width]).astype(BF16))

    def product(weight):
        total = None
        for t in range(n_tp):
            term = jnp.dot(
                scaled[t],
                weight[t * width : (t + 1) * width, :],
                preferred_element_type=F32,
            )
            total = term if total is None else total + term
        return total

    q_wide, v_wide = wq.shape[1], wv.shape[1]
    col = 0
    spans = []
    for weight in (wq, wk, wv, wg):
        acc = product(weight)
        span = (col, col + weight.shape[1])
        spans.append(span)
        for j in range(n_kv):
            part_out[j, :, span[0] : span[1]] = acc[j * seqs : (j + 1) * seqs].astype(BF16)
        col = span[1]
    all_heads = wi.shape[1]
    acc_i = product(wi)
    acc_f = product(wf)
    for j in range(n_kv):
        cut = slice(j * seqs, (j + 1) * seqs)
        gate_out[j] = jnp.zeros((seqs, gate_out.shape[2]), F32)
        gate_out[j, :, 0:all_heads] = acc_i[cut]
        gate_out[j, :, all_heads : 2 * all_heads] = acc_f[cut]
        gate_out[j, :, 2 * all_heads : 2 * all_heads + 1] = squares[cut]
    for dk in far_first(n_kv):
        pk = lax.rem(kv + dk, n_kv)
        for out, into, s_sem, r_sem in (
            (gate_out, gate_in, gate_send, gate_recv),
            (part_out, part_in, part_send, part_recv),
        ):
            copy = remote(out.at[pk], into.at[kv], s_sem.at[dk], r_sem.at[kv], pk, tp)
            copy.start()
            sends.append(copy)
    total = part_out[kv].astype(F32)
    gates = gate_out[kv]
    for copy in get_cell:
        copy.wait()
    for dk in reversed(far_first(n_kv)):
        pk = lax.rem(kv + dk, n_kv)
        remote(gate_out.at[pk], gate_in.at[pk], gate_send.at[dk], gate_recv.at[pk], pk, tp).wait_recv()
        remote(part_out.at[pk], part_in.at[pk], part_send.at[dk], part_recv.at[pk], pk, tp).wait_recv()
        total = total + part_in[pk].astype(F32)
        gates = gates + gate_in[pk]

    row_scale = lax.rsqrt(gates[:, 2 * all_heads : 2 * all_heads + 1] / model_width + EPSILON)
    total = total * row_scale
    queries = total[:, spans[0][0] : spans[0][1]]
    keys_in = total[:, spans[1][0] : spans[1][1]] * (qk**-0.5)
    values_in = total[:, spans[2][0] : spans[2][1]]
    out_pre = total[:, spans[3][0] : spans[3][1]]
    gates = gates * row_scale
    pre_i = gates[:, 0:all_heads] + bias_i[...]
    pre_f = gates[:, all_heads : 2 * all_heads] + bias_f[...]
    log_in = pre_i[:, 0:heads]
    forget_arg = pre_f[:, 0:heads]
    for t in range(1, n_tp):
        log_in = jnp.where(tp == t, pre_i[:, t * heads : (t + 1) * heads], log_in)
        forget_arg = jnp.where(tp == t, pre_f[:, t * heads : (t + 1) * heads], forget_arg)
    log_forget = jnp.minimum(forget_arg, 0.0) - jnp.log1p(jnp.exp(-jnp.abs(forget_arg)))
    carried = log_forget + stab[...]
    stab_now = jnp.maximum(carried, log_in)
    take_new = jnp.exp(log_in - stab_now)
    keep_old = jnp.exp(carried - stab_now)
    stab_out[...] = stab_now
    norm_old = nrm[...]

    q_cols = jnp.transpose(queries)
    for h in range(heads):
        for s in range(seqs):
            column = q_cols[h * qk : (h + 1) * qk, s : s + 1]
            readout[s : s + 1, h * vd : (h + 1) * vd] = jnp.sum(mem[s, h] * column, axis=0, keepdims=True)
    keep_rows, take_rows = [], []
    for h in range(heads):
        k_cut = slice(h * qk, (h + 1) * qk)
        v_cut = slice(h * vd, (h + 1) * vd)
        take = take_new[:, h : h + 1]
        keep = keep_old[:, h : h + 1]
        score = jnp.sum(queries[:, k_cut] * keys_in[:, k_cut], axis=1, keepdims=True)
        past = jnp.sum(norm_old[:, k_cut] * queries[:, k_cut], axis=1, keepdims=True)
        numer = (take * score) * values_in[:, v_cut] + keep * readout[:, v_cut]
        denom = take * score + keep * past
        cell = numer / jnp.maximum(jnp.abs(denom), 1.0)
        hid[me, :, v_cut] = (jax.nn.sigmoid(out_pre[:, v_cut]) * cell).astype(BF16)
        keep_rows.append(jnp.broadcast_to(keep, (seqs, vd)))
        take_rows.append(take * values_in[:, v_cut])
    for i, (dk, dt) in enumerate(offsets):
        pk, pt = peer(dk, dt)
        copy = remote(hid.at[me], hid.at[me], hid_send.at[i], hid_recv.at[me], pk, pt)
        copy.start()
        sends.append(copy)

    k_cols = jnp.transpose(keys_in)
    stores = []
    for s in range(seqs):
        for h in range(heads):
            column = k_cols[h * qk : (h + 1) * qk, s : s + 1]
            mem_out[s, h] = keep_rows[h][s : s + 1] * mem[s, h] + column * take_rows[h][s : s + 1]
    for h in range(heads):
        k_cut = slice(h * qk, (h + 1) * qk)
        nrm_out[:, k_cut] = (
            keep_old[:, h : h + 1] * norm_old[:, k_cut] + take_new[:, h : h + 1] * keys_in[:, k_cut]
        )
    for i, (src, dst) in enumerate(
        [(mem_out, memory_new), (nrm_out, normalizer_new), (stab_out, stabilizer_new)]
    ):
        copy = pltpu.make_async_copy(src, dst, store_sem.at[i])
        copy.start()
        stores.append(copy)

    get_wo.wait()
    for dt in range(1, n_tp):
        pt = lax.rem(tp + dt, n_tp)
        remote(wo.at[pt], wo.at[pt], wo_send.at[dt], wo_recv.at[pt], kv, pt).wait_recv()
    for i, (dk, dt) in reversed(list(enumerate(offsets))):
        pk, pt = peer(dk, dt)
        src = pk * n_tp + pt
        remote(hid.at[src], hid.at[src], hid_send.at[i], hid_recv.at[src], pk, pt).wait_recv()
    projected = None
    for t in range(n_tp):
        lhs = jnp.concatenate([hid[k * n_tp + t].astype(F32) for k in range(n_kv)], axis=0)
        term = jnp.dot(lhs.astype(BF16), wo[t], preferred_element_type=F32)
        projected = term if projected is None else projected + term
    if not aligned:
        picked = projected[:, 0:width]
        for t in range(1, n_tp):
            picked = jnp.where(tp == t, projected[:, t * width : (t + 1) * width], picked)
        projected = picked
    middle = (tok[tp].astype(F32) + projected).astype(BF16)
    mid[me] = middle
    for i, (dk, dt) in enumerate(offsets):
        pk, pt = peer(dk, dt)
        copy = remote(mid.at[me], mid.at[me], mid_send.at[i], mid_recv.at[me], pk, pt)
        copy.start()
        sends.append(copy)

    get_mgain.wait()
    get_up.wait()
    arrivals = [(None, (0, 0))] + list(reversed(list(enumerate(offsets))))
    upward = None
    energy = None
    for i, (dk, dt) in arrivals:
        pk, pt = peer(dk, dt)
        src = pk * n_tp + pt
        if i is not None:
            remote(mid.at[src], mid.at[src], mid_send.at[i], mid_recv.at[src], pk, pt).wait_recv()
        if aligned:
            block = middle.astype(F32) if i is None else mid[src].astype(F32)
            gain = mgain[:, pl.ds(pl.multiple_of(src * width, LANES), width)]
            lhs = (block * gain).astype(BF16)
            weight = wu[pl.ds(pl.multiple_of(src * width, LANES), width), :]
            term = jnp.dot(lhs, weight, preferred_element_type=F32)
            upward = term if upward is None else upward + term
            energy = block * block if energy is None else energy + block * block
    if aligned:
        energy = jnp.sum(energy, axis=1, keepdims=True)
    else:
        for j in range(n_all):
            wide[:, j * width : (j + 1) * width] = mid[j].astype(F32)
        block = wide[...]
        energy = jnp.sum(block * block, axis=1, keepdims=True)
        upward = jnp.dot((block * mgain[...]).astype(BF16), wu[...], preferred_element_type=F32)
    mid_scale = lax.rsqrt(energy / model_width + EPSILON)
    squared = jnp.square(jnp.maximum(upward * mid_scale, 0.0)).astype(BF16)

    get_down.wait()
    if not aligned:
        partial = jnp.dot(squared, wd[...], preferred_element_type=F32)
        for j in range(n_all):
            down_out[j] = partial[:, j * width : (j + 1) * width].astype(BF16)
    for i, (dk, dt) in enumerate(offsets):
        pk, pt = peer(dk, dt)
        dst = pk * n_tp + pt
        if aligned:
            weight = wd[:, pl.ds(pl.multiple_of(dst * width, LANES), width)]
            down_out[dst] = jnp.dot(squared, weight, preferred_element_type=F32).astype(BF16)
        copy = remote(down_out.at[dst], down_in.at[me], down_send.at[i], down_recv.at[me], pk, pt)
        copy.start()
        sends.append(copy)
    if aligned:
        weight = wd[:, pl.ds(pl.multiple_of(me * width, LANES), width)]
        branch = jnp.dot(squared, weight, preferred_element_type=F32)
    else:
        branch = down_out[me].astype(F32)
    branch = branch + middle.astype(F32)
    for i, (dk, dt) in reversed(list(enumerate(offsets))):
        pk, pt = peer(dk, dt)
        src = pk * n_tp + pt
        remote(down_out.at[src], down_in.at[src], down_send.at[i], down_recv.at[src], pk, pt).wait_recv()
        branch = branch + down_in[src].astype(F32)
    mix_out[...] = branch.astype(BF16)
    last = pltpu.make_async_copy(mix_out, mixed_out, store_sem.at[3])
    last.start()
    stores.append(last)
    for copy in sends:
        copy.wait_send()
    for copy in stores:
        copy.wait()


def shards(
    n_kv,
    n_tp,
    tokens,
    norm_gain,
    w_query,
    w_key,
    w_value,
    w_outgate,
    w_ingate,
    w_forget,
    in_bias,
    forget_bias,
    memory,
    normalizer,
    stabilizer,
    w_out,
    mlp_gain,
    w_up,
    w_down,
):
    rows, width = tokens.shape
    seqs, heads, qk, vd = memory.shape
    n_all = n_kv * n_tp
    aligned = width % LANES == 0
    proj = w_query.shape[1] + w_key.shape[1] + w_value.shape[1] + w_outgate.shape[1]
    hidden = heads * vd
    out_cols = width if aligned else w_out.shape[1]
    model_width = mlp_gain.shape[0]
    gate_lanes = -(-(2 * w_ingate.shape[1] + 1) // LANES) * LANES
    operands = (
        tokens,
        norm_gain.reshape(1, -1),
        w_query,
        w_key,
        w_value,
        w_outgate,
        w_ingate,
        w_forget,
        in_bias.reshape(1, -1),
        forget_bias.reshape(1, -1),
        memory,
        normalizer,
        stabilizer,
        w_out,
        mlp_gain.reshape(1, -1),
        w_up,
        w_down,
    )
    anywhere = pl.BlockSpec(memory_space=pl.ANY)

    def like(ref):
        return pltpu.VMEM(ref.shape, ref.dtype)

    dma = pltpu.SemaphoreType.DMA
    scratch = [
        pltpu.VMEM((n_tp, rows, width), BF16),
        like(operands[1]),
        like(w_query),
        like(w_key),
        like(w_value),
        like(w_outgate),
        like(w_ingate),
        like(w_forget),
        like(operands[8]),
        like(operands[9]),
        like(memory),
        like(normalizer),
        like(stabilizer),
        pltpu.VMEM((n_tp, w_out.shape[0], out_cols), BF16),
        like(operands[14]),
        like(w_up),
        like(w_down),
        pltpu.VMEM((n_kv, seqs, proj), BF16),
        pltpu.VMEM((n_kv, seqs, proj), BF16),
        pltpu.VMEM((n_kv, seqs, gate_lanes), F32),
        pltpu.VMEM((n_kv, seqs, gate_lanes), F32),
        pltpu.VMEM((seqs, hidden), F32),
        pltpu.VMEM((n_all, seqs, hidden), BF16),
        pltpu.VMEM((n_all, rows, width), BF16),
        pltpu.VMEM((8, LANES) if aligned else (rows, model_width), F32),
        pltpu.VMEM((n_all, rows, width), BF16),
        pltpu.VMEM((n_all, rows, width), BF16),
        like(memory),
        like(normalizer),
        like(stabilizer),
        like(tokens),
        dma((17,)),
        dma((4,)),
        dma((n_tp,)),
        dma((n_tp,)),
        dma((n_tp,)),
        dma((n_tp,)),
        dma((n_kv,)),
        dma((n_kv,)),
        dma((n_kv,)),
        dma((n_kv,)),
        dma((n_all,)),
        dma((n_all,)),
        dma((n_all,)),
        dma((n_all,)),
        dma((n_all,)),
        dma((n_all,)),
    ]
    return pl.pallas_call(
        functools.partial(step_kernel, n_kv, n_tp),
        out_shape=(
            jax.ShapeDtypeStruct(tokens.shape, tokens.dtype),
            jax.ShapeDtypeStruct(memory.shape, memory.dtype),
            jax.ShapeDtypeStruct(normalizer.shape, normalizer.dtype),
            jax.ShapeDtypeStruct(stabilizer.shape, stabilizer.dtype),
        ),
        in_specs=[anywhere] * len(operands),
        out_specs=(anywhere,) * 4,
        scratch_shapes=scratch,
        compiler_params=pltpu.CompilerParams(
            collective_id=0, has_side_effects=True, vmem_limit_bytes=56 * 1024 * 1024
        ),
    )(*operands)


def solution(mesh):
    placed = (
        P(("grp", "dp"), ("kv", "tp")),
        P("kv"),
        P("kv", "tp"),
        P("kv", "tp"),
        P("kv", "tp"),
        P("kv", "tp"),
        P("kv", None),
        P("kv", None),
        P(),
        P(),
        P(("grp", "dp", "kv"), "tp", None, None),
        P(("grp", "dp", "kv"), "tp"),
        P(("grp", "dp", "kv"), "tp"),
        P("tp", "kv"),
        P(),
        P(None, ("kv", "tp")),
        P(("kv", "tp"), None),
    )
    return jax.shard_map(
        functools.partial(shards, mesh.shape["kv"], mesh.shape["tp"]),
        mesh=mesh,
        in_specs=placed,
        out_specs=(
            P(("grp", "dp"), ("kv", "tp")),
            P(("grp", "dp", "kv"), "tp", None, None),
            P(("grp", "dp", "kv"), "tp"),
            P(("grp", "dp", "kv"), "tp"),
        ),
        check_vma=False,
    )
```

time: 177 us -> 39.8 us (0.22)
  waiting for transfers between devices: 78.4 us -> 0 us
  blocking collectives: 50.2 us -> 0 us
  Pallas kernels: 0 us -> 28.1 us
  matrix products: 18.3 us -> 0 us
  between operations: 14.9 us -> 0.64 us
  other arithmetic: 7.84 us -> 0 us
  local copies, waits for them, and re-layouts: 5.71 us -> 10.6 us
    reduce_scatter x6 -> x0, waiting for transfers between devices: 78.3 us -> none  [the longest x1 30.2 us: shards(): lax.psum_scatter(channel_mix(whole_mid, mlp_gain, w_up, w_down), ('kv', '...]
    all_gather x3 -> x0, blocking collectives: 29.7 us -> none  [the longest x1 14.2 us: shards(): whole_mid = lax.all_gather(middle, ('kv', 'tp'), axis=1, tiled=True)]
    pallas_call x0 -> x1, Pallas kernels: none -> 28.1 us  [shards(): pl.pallas_call(functools.partial(step_kernel, n_kv, n_tp), out_shape=(jax...]
    unnamed x1 -> x0, blocking collectives: 20.5 us -> none
    dot_general x9 -> x0, matrix products: 18.3 us -> none  [the longest x6 8.49 us: product(): jnp.dot(scaled, weight, preferred_element_type=jnp.float32)]
    unnamed x11 -> x6, local copies, waits for them, and re-layouts: 2.67 us -> 9.24 us
    convert_element_type x5 -> x0, other arithmetic: 2.86 us -> none  [the longest x1 1.33 us: shards(): mixed_out = (middle.astype(jnp.float32) + branch).astype(jnp.bfloat16)]
    add x2 -> x0, other arithmetic: 2.74 us -> none  [the longest x1 1.38 us: shards(): keep_old[..., None] * norm_old + take_new[..., None] * keys_in]
  transfers between devices with their start and end apart: 6 -> 0, of which waited for: 5 -> 0; matrix products, arithmetic and copies ran while one was open for 11% -> 0% of each run, Pallas kernels for 0% -> 0%
where the time goes in v1:
time: 39.8 us; the launch traced here: 39.3 us
  Pallas kernels  28.1 us (71%)
  local copies, waits for them, and re-layouts  10.6 us (27%)
  between operations  0.64 us (2%)
    pallas_call x1, Pallas kernels, shards(): pl.pallas_call(functools.partial(step_kernel, n_kv, n_tp), out_shape=(jax...  28.1 us
    unnamed x6, local copies, waits for them, and re-layouts  9.24 us
    pallas_call x1, local copies, waits for them, and re-layouts, shards(): pl.pallas_call(functools.partial(step_kernel, n_kv, n_tp), out_shape=(jax...  1.33 us

profile of v1, /device:TPU:0, one launch (start us, length us, event | category | flops | bytes accessed | tf_op | source)
XLA Modules:
  0.0 39.3 jit_solution(9275968569159254767)
XLA Ops:
  0.6 1.3 %copy.23.stabilizer = f32[8,4]{1,0:T(8,128)} copy(f32[8,4]{0,1:T(4,128)} %param.29) | data formatting | bytes 256 | tf_op args[12]
  2.0 1.5 %copy.21.w_ingate = bf16[512,8]{1,0:T(8,128)(2,1)} copy(bf16[512,8]{0,1:T(8,128)(2,1)} %param.23) | data formatting | bytes 16384 | tf_op args[6]
  3.5 1.5 %copy.22.w_forget = bf16[512,8]{1,0:T(8,128)(2,1)} copy(bf16[512,8]{0,1:T(8,128)(2,1)} %param.24) | data formatting | bytes 16384 | tf_op args[7]
  5.0 28.1 %shard_map.192 = (bf16[32,256]{1,0:T(8,128)(2,1)}, f32[8,4,64,128]{3,2,1,0:T(8,128)}, f32[8,256]{1,0:T(8,128)}, f32[8,4]{1,0:T(8,128)}) custom-call(bf16[32,256]{1,0:T(8,128)(2,1)} %tokens.1, f32[1,512]{1,0:T(1,128)} %bitcast.5, bf16[512,256]{1,0:T(8,128)(2,1)} %w_query.1, bf16[512,256]{1,0:T(8,128)(2,1)} %w_key.1, bf16[512,512]{1,0:T(8,128)(2,1)} %w_value.1, ...), custom_call_target="tpu_custom_call" | custom-call | tf_op jit(solution)/shard_map/pallas_call | solution.py:505
  33.0 1.3 %copy.24 = f32[8,4]{0,1:T(4,128)} copy(f32[8,4]{1,0:T(8,128)} %get-tuple-element.7) | data formatting | bytes 256 | tf_op jit(solution)/shard_map/pallas_call | solution.py:505
  34.4 1.3 %copy.28 = bf16[32,256]{1,0:T(8,128)(2,1)} copy(bf16[32,256]{1,0:T(8,128)(2,1)} %get-tuple-element.12) | data formatting | bytes 32768
  35.7 2.3 %copy.29 = f32[8,4,64,128]{3,2,1,0:T(8,128)} copy(f32[8,4,64,128]{3,2,1,0:T(8,128)} %get-tuple-element.13) | data formatting | bytes 2097152
  38.0 1.3 %copy.30 = f32[8,256]{1,0:T(8,128)} copy(f32[8,256]{1,0:T(8,128)} %get-tuple-element.14) | data formatting | bytes 16384

commit v2 on v1

--- a/solution.py
+++ b/solution.py
@@ -61,6 +61,8 @@
     wd,
     part_out,
     part_in,
+    late_out,
+    late_in,
     gate_out,
     gate_in,
     readout,
@@ -69,18 +71,15 @@
     wide,
     down_out,
     down_in,
-    mem_out,
-    nrm_out,
-    stab_out,
-    mix_out,
     load_sem,
-    store_sem,
     tok_send,
     tok_recv,
     wo_send,
     wo_recv,
     part_send,
     part_recv,
+    late_send,
+    late_recv,
     gate_send,
     gate_recv,
     hid_send,
@@ -204,51 +203,62 @@
             total = term if total is None else total + term
         return total
 
-    q_wide, v_wide = wq.shape[1], wv.shape[1]
-    col = 0
-    spans = []
-    for weight in (wq, wk, wv, wg):
-        acc = product(weight)
-        span = (col, col + weight.shape[1])
-        spans.append(span)
-        for j in range(n_kv):
-            part_out[j, :, span[0] : span[1]] = acc[j * seqs : (j + 1) * seqs].astype(BF16)
-        col = span[1]
-    all_heads = wi.shape[1]
-    acc_i = product(wi)
-    acc_f = product(wf)
+    def turned(weight):
+        total = None
+        for t in range(n_tp):
+            term = lax.dot_general(
+                scaled[t],
+                weight[:, t * width : (t + 1) * width],
+                (((1,), (1,)), ((), ())),
+                preferred_element_type=F32,
+            )
+            total = term if total is None else total + term
+        return total
+
+    def scatter(out, into, s_sem, r_sem):
+        for dk in far_first(n_kv):
+            pk = lax.rem(kv + dk, n_kv)
+            copy = remote(out.at[pk], into.at[kv], s_sem.at[dk], r_sem.at[kv], pk, tp)
+            copy.start()
+            sends.append(copy)
+
+    def collect(total, out, into, s_sem, r_sem):
+        for dk in reversed(far_first(n_kv)):
+            pk = lax.rem(kv + dk, n_kv)
+            remote(out.at[pk], into.at[pk], s_sem.at[dk], r_sem.at[pk], pk, tp).wait_recv()
+            total = total + into[pk].astype(F32)
+        return total
+
+    all_heads = wi.shape[0]
+    acc_i = turned(wi)
+    acc_f = turned(wf)
     for j in range(n_kv):
         cut = slice(j * seqs, (j + 1) * seqs)
-        gate_out[j] = jnp.zeros((seqs, gate_out.shape[2]), F32)
         gate_out[j, :, 0:all_heads] = acc_i[cut]
         gate_out[j, :, all_heads : 2 * all_heads] = acc_f[cut]
         gate_out[j, :, 2 * all_heads : 2 * all_heads + 1] = squares[cut]
-    for dk in far_first(n_kv):
-        pk = lax.rem(kv + dk, n_kv)
-        for out, into, s_sem, r_sem in (
-            (gate_out, gate_in, gate_send, gate_recv),
-            (part_out, part_in, part_send, part_recv),
-        ):
-            copy = remote(out.at[pk], into.at[kv], s_sem.at[dk], r_sem.at[kv], pk, tp)
-            copy.start()
-            sends.append(copy)
-    total = part_out[kv].astype(F32)
-    gates = gate_out[kv]
+    scatter(gate_out, gate_in, gate_send, gate_recv)
+    for weights, out in (((wq, wk), part_out), ((wv, wg), late_out)):
+        col = 0
+        for weight in weights:
+            acc = product(weight)
+            end = col + weight.shape[1]
+            for j in range(n_kv):
+                out[j, :, col:end] = acc[j * seqs : (j + 1) * seqs].astype(BF16)
+            col = end
+        if out is part_out:
+            scatter(part_out, part_in, part_send, part_recv)
+        else:
+            scatter(late_out, late_in, late_send, late_recv)
     for copy in get_cell:
         copy.wait()
-    for dk in reversed(far_first(n_kv)):
-        pk = lax.rem(kv + dk, n_kv)
-        remote(gate_out.at[pk], gate_in.at[pk], gate_send.at[dk], gate_recv.at[pk], pk, tp).wait_recv()
-        remote(part_out.at[pk], part_in.at[pk], part_send.at[dk], part_recv.at[pk], pk, tp).wait_recv()
-        total = total + part_in[pk].astype(F32)
-        gates = gates + gate_in[pk]
+    gates = collect(gate_out[kv], gate_out, gate_in, gate_send, gate_recv)
+    early = collect(part_out[kv].astype(F32), part_out, part_in, part_send, part_recv)
 
     row_scale = lax.rsqrt(gates[:, 2 * all_heads : 2 * all_heads + 1] / model_width + EPSILON)
-    total = total * row_scale
-    queries = total[:, spans[0][0] : spans[0][1]]
-    keys_in = total[:, spans[1][0] : spans[1][1]] * (qk**-0.5)
-    values_in = total[:, spans[2][0] : spans[2][1]]
-    out_pre = total[:, spans[3][0] : spans[3][1]]
+    early = early * row_scale
+    queries = early[:, 0 : heads * qk]
+    keys_in = early[:, heads * qk :] * (qk**-0.5)
     gates = gates * row_scale
     pre_i = gates[:, 0:all_heads] + bias_i[...]
     pre_f = gates[:, all_heads : 2 * all_heads] + bias_f[...]
@@ -258,11 +268,11 @@
         log_in = jnp.where(tp == t, pre_i[:, t * heads : (t + 1) * heads], log_in)
         forget_arg = jnp.where(tp == t, pre_f[:, t * heads : (t + 1) * heads], forget_arg)
     log_forget = jnp.minimum(forget_arg, 0.0) - jnp.log1p(jnp.exp(-jnp.abs(forget_arg)))
-    carried = log_forget + stab[...]
+    carried = log_forget + jnp.transpose(stab[...])
     stab_now = jnp.maximum(carried, log_in)
     take_new = jnp.exp(log_in - stab_now)
     keep_old = jnp.exp(carried - stab_now)
-    stab_out[...] = stab_now
+    stabilizer_new[...] = jnp.transpose(stab_now)
     norm_old = nrm[...]
 
     q_cols = jnp.transpose(queries)
@@ -270,6 +280,10 @@
         for s in range(seqs):
             column = q_cols[h * qk : (h + 1) * qk, s : s + 1]
             readout[s : s + 1, h * vd : (h + 1) * vd] = jnp.sum(mem[s, h] * column, axis=0, keepdims=True)
+    late = collect(late_out[kv].astype(F32), late_out, late_in, late_send, late_recv)
+    late = late * row_scale
+    values_in = late[:, 0 : heads * vd]
+    out_pre = late[:, heads * vd :]
     keep_rows, take_rows = [], []
     for h in range(heads):
         k_cut = slice(h * qk, (h + 1) * qk)
@@ -291,23 +305,15 @@
         sends.append(copy)
 
     k_cols = jnp.transpose(keys_in)
-    stores = []
     for s in range(seqs):
         for h in range(heads):
             column = k_cols[h * qk : (h + 1) * qk, s : s + 1]
-            mem_out[s, h] = keep_rows[h][s : s + 1] * mem[s, h] + column * take_rows[h][s : s + 1]
+            memory_new[s, h] = keep_rows[h][s : s + 1] * mem[s, h] + column * take_rows[h][s : s + 1]
     for h in range(heads):
         k_cut = slice(h * qk, (h + 1) * qk)
-        nrm_out[:, k_cut] = (
+        normalizer_new[:, k_cut] = (
             keep_old[:, h : h + 1] * norm_old[:, k_cut] + take_new[:, h : h + 1] * keys_in[:, k_cut]
         )
-    for i, (src, dst) in enumerate(
-        [(mem_out, memory_new), (nrm_out, normalizer_new), (stab_out, stabilizer_new)]
-    ):
-        copy = pltpu.make_async_copy(src, dst, store_sem.at[i])
-        copy.start()
-        stores.append(copy)
-
     get_wo.wait()
     for dt in range(1, n_tp):
         pt = lax.rem(tp + dt, n_tp)
@@ -388,13 +394,20 @@
         src = pk * n_tp + pt
         remote(down_out.at[src], down_in.at[src], down_send.at[i], down_recv.at[src], pk, pt).wait_recv()
         branch = branch + down_in[src].astype(F32)
-    mix_out[...] = branch.astype(BF16)
-    last = pltpu.make_async_copy(mix_out, mixed_out, store_sem.at[3])
-    last.start()
-    stores.append(last)
+    mixed_out[...] = branch.astype(BF16)
     for copy in sends:
         copy.wait_send()
-    for copy in stores:
+
+
+def store_kernel(*refs):
+    count = (len(refs) - 1) // 2
+    sem = refs[-1]
+    copies = [
+        pltpu.make_async_copy(refs[i], refs[count + i], sem.at[i]) for i in range(count)
+    ]
+    for copy in copies:
+        copy.start()
+    for copy in copies:
         copy.wait()
 
 
@@ -423,7 +436,8 @@
     seqs, heads, qk, vd = memory.shape
     n_all = n_kv * n_tp
     aligned = width % LANES == 0
-    proj = w_query.shape[1] + w_key.shape[1] + w_value.shape[1] + w_outgate.shape[1]
+    early = w_query.shape[1] + w_key.shape[1]
+    late = w_value.shape[1] + w_outgate.shape[1]
     hidden = heads * vd
     out_cols = width if aligned else w_out.shape[1]
     model_width = mlp_gain.shape[0]
@@ -435,13 +449,13 @@
         w_key,
         w_value,
         w_outgate,
-        w_ingate,
-        w_forget,
+        w_ingate.T,
+        w_forget.T,
         in_bias.reshape(1, -1),
         forget_bias.reshape(1, -1),
         memory,
         normalizer,
-        stabilizer,
+        stabilizer.T,
         w_out,
         mlp_gain.reshape(1, -1),
         w_up,
@@ -460,19 +474,21 @@
         like(w_key),
         like(w_value),
         like(w_outgate),
-        like(w_ingate),
-        like(w_forget),
+        like(operands[6]),
+        like(operands[7]),
         like(operands[8]),
         like(operands[9]),
         like(memory),
         like(normalizer),
-        like(stabilizer),
+        like(operands[12]),
         pltpu.VMEM((n_tp, w_out.shape[0], out_cols), BF16),
         like(operands[14]),
         like(w_up),
         like(w_down),
-        pltpu.VMEM((n_kv, seqs, proj), BF16),
-        pltpu.VMEM((n_kv, seqs, proj), BF16),
+        pltpu.VMEM((n_kv, seqs, early), BF16),
+        pltpu.VMEM((n_kv, seqs, early), BF16),
+        pltpu.VMEM((n_kv, seqs, late), BF16),
+        pltpu.VMEM((n_kv, seqs, late), BF16),
         pltpu.VMEM((n_kv, seqs, gate_lanes), F32),
         pltpu.VMEM((n_kv, seqs, gate_lanes), F32),
         pltpu.VMEM((seqs, hidden), F32),
@@ -481,16 +497,13 @@
         pltpu.VMEM((8, LANES) if aligned else (rows, model_width), F32),
         pltpu.VMEM((n_all, rows, width), BF16),
         pltpu.VMEM((n_all, rows, width), BF16),
-        like(memory),
-        like(normalizer),
-        like(stabilizer),
-        like(tokens),
         dma((17,)),
-        dma((4,)),
         dma((n_tp,)),
         dma((n_tp,)),
         dma((n_tp,)),
         dma((n_tp,)),
+        dma((n_kv,)),
+        dma((n_kv,)),
         dma((n_kv,)),
         dma((n_kv,)),
         dma((n_kv,)),
@@ -502,21 +515,29 @@
         dma((n_all,)),
         dma((n_all,)),
     ]
-    return pl.pallas_call(
+    shapes = tuple(
+        jax.ShapeDtypeStruct(a.shape, a.dtype)
+        for a in (tokens, memory, normalizer, operands[12])
+    )
+    in_vmem = (pl.BlockSpec(memory_space=pltpu.VMEM),) * len(shapes)
+    held = pl.pallas_call(
         functools.partial(step_kernel, n_kv, n_tp),
-        out_shape=(
-            jax.ShapeDtypeStruct(tokens.shape, tokens.dtype),
-            jax.ShapeDtypeStruct(memory.shape, memory.dtype),
-            jax.ShapeDtypeStruct(normalizer.shape, normalizer.dtype),
-            jax.ShapeDtypeStruct(stabilizer.shape, stabilizer.dtype),
-        ),
+        out_shape=tuple(pltpu.VMEM(a.shape, a.dtype) for a in shapes),
         in_specs=[anywhere] * len(operands),
-        out_specs=(anywhere,) * 4,
+        out_specs=in_vmem,
         scratch_shapes=scratch,
         compiler_params=pltpu.CompilerParams(
             collective_id=0, has_side_effects=True, vmem_limit_bytes=56 * 1024 * 1024
         ),
     )(*operands)
+    mixed_out, memory_new, normalizer_new, stab_new = pl.pallas_call(
+        store_kernel,
+        out_shape=shapes,
+        in_specs=in_vmem,
+        out_specs=(anywhere,) * len(shapes),
+        scratch_shapes=[dma((len(shapes),))],
+    )(*[pltpu.with_memory_space_constraint(a, pltpu.VMEM) for a in held])
+    return (mixed_out, memory_new, normalizer_new, stab_new.T)
 
 
 def solution(mesh):

time: 39.8 us -> 28.7 us (0.72)
  local copies, waits for them, and re-layouts: 10.6 us -> 0 us
    unnamed x6 -> x0, local copies, waits for them, and re-layouts: 9.24 us -> none
    pallas_call x1 -> x0, local copies, waits for them, and re-layouts: 1.33 us -> none  [shards(): pl.pallas_call(functools.partial(step_kernel, n_kv, n_tp), out_shape=(jax...]
    pallas_call x1 -> x2, Pallas kernels: 28.1 us -> 27.8 us  [the longest x1 26.8 us: shards(): pl.pallas_call(functools.partial(step_kernel, n_kv, n_tp), out_shape=tupl...]
where the time goes in v2:
time: 28.7 us; the launch traced here: 28.5 us
  Pallas kernels  27.8 us (97%)
  between operations  0.65 us (2%)
    pallas_call x1, Pallas kernels, shards(): pl.pallas_call(functools.partial(step_kernel, n_kv, n_tp), out_shape=tupl...  26.8 us
    pallas_call x1, Pallas kernels, shards(): pl.pallas_call(store_kernel, out_shape=shapes, in_specs=in_vmem, out_spec...  1.02 us

profile of v2, /device:TPU:0, one launch (start us, length us, event | category | flops | bytes accessed | tf_op | source)
XLA Modules:
  0.0 28.5 jit_solution(12124220156053642275)
XLA Ops:
  0.6 26.8 %shard_map.192 = (bf16[32,256]{1,0:T(8,128)(2,1)S(1)}, f32[8,4,64,128]{3,2,1,0:T(8,128)S(1)}, f32[8,256]{1,0:T(8,128)S(1)}, f32[4,8]{1,0:T(4,128)S(1)}) custom-call(bf16[32,256]{1,0:T(8,128)(2,1)} %tokens.1, f32[1,512]{1,0:T(1,128)} %bitcast.11, bf16[512,256]{1,0:T(8,128)(2,1)} %w_query.1, bf16[512,256]{1,0:T(8,128)(2,1)} %w_key.1, ...), custom_call_target="tpu_custom_call" | custom-call | tf_op jit(solution)/shard_map/pallas_call | solution.py:523
  27.5 1.0 %shard_map.193 = (bf16[32,256]{1,0:T(8,128)(2,1)}, f32[8,4,64,128]{3,2,1,0:T(8,128)}, f32[8,256]{1,0:T(8,128)}, f32[4,8]{1,0:T(4,128)}) custom-call(bf16[32,256]{1,0:T(8,128)(2,1)S(1)} %get-tuple-element.12.refs_0_, f32[8,4,64,128]{3,2,1,0:T(8,128)S(1)} %get-tuple-element.13.refs_1_, f32[8,256]{1,0:T(8,128)S(1)} %get-tuple-element.14.refs_2_, ...), custom_call_target="tpu_custom_call" | custom-call | tf_op jit(solution)/shard_map/pallas_call | solution.py:533
